TPU v7x, 32 devices: a whole 2x2x4 slice. The times are simulated.
32 devices in a mesh: sp: 8 (over z, y), tp: 4 (over x, core).
Axes of the slice: x: 2, y: 2, z: 4, core: 2. Of those that a mesh axis runs over, the one named last changes fastest.
Arguments:
- stream: bfloat16 [3072, 2048], P(('sp', 'tp')), may hold values from -6 to 6
- query_projected: bfloat16 [3072, 1024], P('sp', 'tp'), may hold values from -6 to 6
- key_projected: bfloat16 [3072, 1024], P('sp', 'tp'), may hold values from -6 to 6
- value_projected: bfloat16 [3072, 1024], P('sp', 'tp'), may hold values from -6 to 6
- gate_projected: bfloat16 [3072, 1024], P('sp', 'tp'), may hold values from -6 to 6
- strength_logits: bfloat16 [8, 3072], P('tp', 'sp'), may hold values from -7 to 4
- decay_preactivation: bfloat16 [8, 3072], P('tp', 'sp'), may hold values from -9 to 9
- extra_log_decay: float32 [8, 3072], P('tp', 'sp'), may hold values from -0.7 to 0
- head_decay_rate: float32 [8], P('tp'), may hold values from 0 to 0.1
- head_norm_gain: float32 [128], replicated, may hold values from 0.1 to 1.9
- head_output_matrix: bfloat16 [1024, 2048], P('tp'), may hold values from -0.1875 to 0.1875
- feed_norm_gain: float32 [2048], replicated, may hold values from 0.1 to 1.9
- gate_matrix: bfloat16 [2048, 5632], P('sp', 'tp'), may hold values from -0.125 to 0.125
- up_matrix: bfloat16 [2048, 5632], P('sp', 'tp'), may hold values from -0.125 to 0.125
- down_matrix: bfloat16 [5632, 2048], P('tp', 'sp'), may hold values from -0.078125 to 0.078125
Outputs:
- result: bfloat16 [3072, 2048], P(('sp', 'tp'))
All inputs are finite; a program needn't handle non-finite values.
Results may differ from a plain program's by a relative error of at most 0.015.
Values may be sent and summed in bfloat16 or wider, within the bound.
No kernel may reach another device: no remote copies, remote signals or barrier semaphores. Data moves between devices by JAX's collectives and lax.ppermute only.
A program may use at most 128 MiB of HBM per device.

v0:
```python
import jax
import jax.numpy as jnp
from jax import lax
from jax.sharding import PartitionSpec as P

HEAD = 128
BLOCK = 64
PRECISION_FULL = lax.Precision.HIGHEST
EPSILON = 1e-06


def from_behind(value, axis, by):
    size = lax.axis_size(axis)
    pairs = [(i, i + by) for i in range(size) if 0 <= i + by < size]
    return lax.ppermute(value, axis, pairs)


def unit_rows(tensor):
    return tensor * lax.rsqrt(jnp.sum(tensor * tensor, axis=-1, keepdims=True) + EPSILON)


def rms_scale(tensor):
    return tensor * lax.rsqrt(jnp.mean(tensor * tensor, axis=-1, keepdims=True) + EPSILON)


def block_correction(
    unit_queries,
    unit_keys,
    complete_values,
    strength_logits,
    decay_preactivation,
    extra_log_decay,
    head_decay_rate,
):
    head_count, length, head_width = unit_queries.shape
    block_count = length // BLOCK

    def to_blocks(tensor):
        return tensor.reshape((head_count, block_count, BLOCK) + tensor.shape[2:])

    beta_gate = jax.nn.sigmoid(strength_logits.astype(jnp.float32))
    decay_logarithm = (
        -head_decay_rate[:, None] * jax.nn.softplus(decay_preactivation.astype(jnp.float32))
        + extra_log_decay
    )
    query_block = to_blocks(unit_queries)
    key_block = to_blocks(unit_keys)
    value_block = to_blocks(complete_values)
    beta_block = to_blocks(beta_gate)
    cumulative = jnp.cumsum(to_blocks(decay_logarithm), axis=-1)
    causal = jnp.tril(jnp.ones((BLOCK, BLOCK), bool))
    strict = jnp.tril(jnp.ones((BLOCK, BLOCK), bool), -1)
    spread = cumulative[..., :, None] - cumulative[..., None, :]
    damping = jnp.where(causal, jnp.exp(jnp.where(causal, spread, 0.0)), 0.0)
    key_beta = key_block * beta_block[..., None]
    lower_part = jnp.einsum(
        "hnid,hnjd->hnij", key_beta, key_block, precision=PRECISION_FULL
    ) * jnp.where(strict, damping, 0.0)
    system = lower_part + jnp.eye(BLOCK, dtype=jnp.float32)
    right_side = jnp.concatenate(
        [value_block * beta_block[..., None], key_beta * jnp.exp(cumulative)[..., None]], axis=-1
    )
    solved = lax.linalg.triangular_solve(
        system, right_side, left_side=True, lower=True, unit_diagonal=True
    )
    target_values = solved[..., :head_width]
    householder_weights = solved[..., head_width:]
    inner_scores = (
        jnp.einsum("hnid,hnjd->hnij", query_block, key_block, precision=PRECISION_FULL) * damping
    )
    decayed_queries = query_block * jnp.exp(cumulative)[..., None]
    closing_log_decay = cumulative[..., -1:]
    decayed_keys = key_block * jnp.exp(closing_log_decay - cumulative)[..., None]
    return (
        decayed_queries,
        decayed_keys,
        target_values,
        householder_weights,
        inner_scores,
        closing_log_decay,
    )


def local_recurrence(
    query_projected,
    key_projected,
    value_projected,
    strength_logits,
    decay_preactivation,
    extra_log_decay,
    head_decay_rate,
):
    head_count = strength_logits.shape[0]
    tok_count = strength_logits.shape[1]

    def split_heads(tensor):
        return tensor.reshape(tok_count, head_count, HEAD).transpose(1, 0, 2).astype(jnp.float32)

    unit_queries = unit_rows(split_heads(query_projected)) * HEAD ** (-0.5)
    unit_keys = unit_rows(split_heads(key_projected))
    complete_values = split_heads(value_projected)
    score_terms = block_correction(
        unit_queries,
        unit_keys,
        complete_values,
        strength_logits,
        decay_preactivation,
        extra_log_decay,
        head_decay_rate,
    )
    identity = jnp.broadcast_to(jnp.eye(HEAD, dtype=jnp.float32), (head_count, HEAD, HEAD))

    def advance(carry, items):
        running_state, matrix_product = carry
        (
            decayed_queries,
            decayed_keys,
            target_values,
            householder_weights,
            inner_scores,
            closing_log_decay,
        ) = items
        new_state = target_values - jnp.einsum(
            "fdc,fcj->fdj", householder_weights, running_state, precision=PRECISION_FULL
        )
        layer_output = jnp.einsum(
            "fdc,fcj->fdj", decayed_queries, running_state, precision=PRECISION_FULL
        )
        layer_output = layer_output + jnp.einsum(
            "hij,hjv->hiv", inner_scores, new_state, precision=PRECISION_FULL
        )
        passed_state = decayed_queries - jnp.einsum(
            "hij,hjk->hik", inner_scores, householder_weights, precision=PRECISION_FULL
        )
        decay_span = jnp.einsum(
            "fdc,fcj->fdj", passed_state, matrix_product, precision=PRECISION_FULL
        )
        decay_factor = jnp.exp(closing_log_decay)[:, :, None]
        step_map = decay_factor * identity - jnp.einsum(
            "hik,hij->hkj", decayed_keys, householder_weights, precision=PRECISION_FULL
        )
        running_state = decay_factor * running_state + jnp.einsum(
            "xwp,xws->xps", decayed_keys, new_state, precision=PRECISION_FULL
        )
        matrix_product = jnp.einsum(
            "hij,hjk->hik", step_map, matrix_product, precision=PRECISION_FULL
        )
        return ((running_state, matrix_product), (layer_output, decay_span))

    moved = tuple((jnp.moveaxis(tensor, 1, 0) for tensor in score_terms))
    zeros_state = jnp.zeros((head_count, HEAD, HEAD), jnp.float32)
    (running_state, matrix_product), (block_outputs, decay_spans) = lax.scan(
        advance, (zeros_state, identity), moved
    )

    def merge_blocks(tensor):
        return jnp.moveaxis(tensor, 0, 1).reshape(head_count, tok_count, HEAD)

    return (
        merge_blocks(block_outputs),
        merge_blocks(decay_spans),
        matrix_product,
        running_state,
        identity,
    )


def feed_forward(whole_rows, gate_matrix, up_matrix, down_matrix):
    gate_whole, up_whole = (
        lax.all_gather(gate_matrix, "sp", axis=0, tiled=True),
        lax.all_gather(up_matrix, "sp", axis=0, tiled=True),
    )
    gate_total = jnp.dot(whole_rows, gate_whole, preferred_element_type=jnp.float32)
    up_total = jnp.dot(whole_rows, up_whole, preferred_element_type=jnp.float32)
    hidden = (jax.nn.silu(gate_total) * up_total).astype(jnp.bfloat16)
    down_whole = lax.all_gather(down_matrix, "sp", axis=1, tiled=True)
    return jnp.dot(hidden, down_whole, preferred_element_type=jnp.float32)


def body(
    stream,
    query_projected,
    key_projected,
    value_projected,
    gate_projected,
    strength_logits,
    decay_preactivation,
    extra_log_decay,
    head_decay_rate,
    head_norm_gain,
    head_output_matrix,
    feed_norm_gain,
    gate_matrix,
    up_matrix,
    down_matrix,
):
    block_outputs, decay_spans, matrix_product, running_state, identity = local_recurrence(
        query_projected,
        key_projected,
        value_projected,
        strength_logits,
        decay_preactivation,
        extra_log_decay,
        head_decay_rate,
    )
    zeros_state = jnp.zeros_like(running_state)

    def pass_state(turn, state_inflow):
        leaving = (
            jnp.einsum("hij,hjk->hik", matrix_product, state_inflow, precision=PRECISION_FULL)
            + running_state
        )
        return from_behind(leaving.astype(jnp.bfloat16), "sp", 1).astype(leaving.dtype)

    state_inflow = lax.fori_loop(0, lax.axis_size("sp") - 1, pass_state, zeros_state)
    attention_output = block_outputs + jnp.einsum(
        "qwc,qcn->qwn", decay_spans, state_inflow, precision=PRECISION_FULL
    )
    head_count = attention_output.shape[0]
    tok_count = attention_output.shape[1]
    normed_heads = rms_scale(attention_output) * head_norm_gain
    gated = normed_heads.transpose(1, 0, 2).reshape(tok_count, head_count * HEAD)
    mixed = (gated * jax.nn.silu(gate_projected.astype(jnp.float32))).astype(jnp.bfloat16)
    branch = lax.psum_scatter(
        jnp.dot(mixed, head_output_matrix, preferred_element_type=jnp.float32).astype(jnp.bfloat16),
        "tp",
        scatter_dimension=0,
        tiled=True,
    ).astype(jnp.float32)
    residual_own = stream.astype(jnp.float32) + branch
    normed_own = (rms_scale(residual_own) * feed_norm_gain).astype(jnp.bfloat16)
    whole_rows = lax.all_gather(normed_own, "tp", axis=0, tiled=True)
    ffn_term = feed_forward(whole_rows, gate_matrix, up_matrix, down_matrix)
    ffn_own = lax.psum_scatter(
        ffn_term.astype(jnp.bfloat16), "tp", scatter_dimension=0, tiled=True
    ).astype(jnp.float32)
    return (residual_own + ffn_own).astype(jnp.bfloat16)


def solution(mesh):
    placed = (
        P(("sp", "tp"), None),
        P("sp", "tp"),
        P("sp", "tp"),
        P("sp", "tp"),
        P("sp", "tp"),
        P("tp", "sp"),
        P("tp", "sp"),
        P("tp", "sp"),
        P("tp"),
        P(),
        P("tp", None),
        P(),
        P("sp", "tp"),
        P("sp", "tp"),
        P("tp", "sp"),
    )
    return jax.shard_map(
        body, mesh=mesh, in_specs=placed, out_specs=P(("sp", "tp"), None), check_vma=False
    )
```

profile of v0, /device:TPU:0, one launch (start us, length us, event | category | flops | bytes accessed | tf_op | source)
XLA Modules:
  0.0 551.2 jit_solution(7347479485389619198)
XLA Ops:
  8.9 1.1 fusion.64
  10.0 1.1 fusion.62
  11.1 1.1 fusion.60
  12.2 1.1 fusion.61
  14.1 1.0 copy_bitcast_fusion
  16.0 59.6 %custom-call.3 = f32[2,6,1,64,64]{3,4,2,1,0:T(8,128)} custom-call(f32[2,6,1,64,64]{4,3,2,1,0:T(8,128)S(1)} %fusion.48), custom_call_target="InvertDiagBlocksLowerTriangular" | custom-call | tf_op jit(solution)/shard_map/triangular_solve | solution.py:63
  75.6 1.1 multiply_multiply_fusion
  76.7 0.9 fusion.49
  77.6 0.8 slice_bitcast_fusion
  79.3 36.4 %while.28 = (s32[]{:T(128)}, f32[2,128,128]{2,1,0:T(8,128)S(1)}, f32[2,128,128]{2,1,0:T(8,128)S(1)}, f32[6,2,64,128]{3,2,0,1:T(8,128)}, f32[6,2,64,128]{3,2,0,1:...) while((s32[]{:T(128)}, f32[2,128,128]{2,1,0:T(8,128)S(1)}, ...), condition=%wide.region_4.5_spmd.clone, body=%wide.region_3.4_spmd.clone.sunk | while | flops 201605120 | bytes 2759337 | solution.py:152
  79.4 1.1 convolution_subtract_fusion.6
  80.5 1.1 fusion.145
  81.5 0.8 fusion.146
  82.8 1.0 convolution_subtract_fusion.8
  83.9 0.9 fusion.147
  85.4 1.1 convolution_subtract_fusion.6
  86.5 1.1 fusion.145
  87.6 0.8 fusion.146
  88.9 1.0 convolution_subtract_fusion.8
  89.9 0.9 fusion.147
  91.5 1.1 convolution_subtract_fusion.6
  92.6 1.1 fusion.145
  94.9 1.0 convolution_subtract_fusion.8
  96.0 0.9 fusion.147
  97.5 1.1 convolution_subtract_fusion.6
  98.6 1.1 fusion.145
  101.0 1.0 convolution_subtract_fusion.8
  102.0 0.9 fusion.147
  103.6 1.1 convolution_subtract_fusion.6
  104.7 1.1 fusion.145
  107.0 1.0 convolution_subtract_fusion.8
  108.1 0.9 fusion.147
  109.7 1.1 convolution_subtract_fusion.6
  110.7 1.1 fusion.145
  113.1 1.0 convolution_subtract_fusion.8
  114.2 0.9 fusion.147
  115.7 1.2 copy.42
  116.9 49.8 %while.29 = (s32[]{:T(128)}, f32[2,128,128]{2,1,0:T(8,128)S(1)}, f32[2,128,128]{2,1,0:T(8,128)S(1)}, f32[2,128,128]{2,1,0:T(8,128)S(1)}, s32[]{:T(128)}, /*index=5*/s32[]{:T(128)}) while((s32[]{:T(128)}, f32[2,128,128]{2,1,0:T(8,128)S(1)}, f32[2,128,128]{2,1,0:T(8,128)S(1)}, f32[2,128,128]{2,1,0:T(8,128)S(1)}, s32[]{:T(128)}, ...), condition=%wide.region_6.7_spmd.clone, body=%wide.region_5.6_spmd.clone.sunk | while | flops 50462720 | bytes 917623 | solution.py:215
  117.2 4.9 collective-permute-start
  122.1 1.9 collective-permute-done
  124.3 4.3 collective-permute-start
  128.6 1.9 collective-permute-done
  130.8 4.3 collective-permute-start
  135.1 1.9 collective-permute-done
  137.3 5.2 collective-permute-start
  142.5 1.9 collective-permute-done
  144.7 5.2 collective-permute-start
  149.9 1.9 collective-permute-done
  152.1 5.3 collective-permute-start
  157.3 2.1 collective-permute-done
  159.7 5.1 collective-permute-start
  164.8 1.9 collective-permute-done
  167.8 1.8 convolution_convert_fusion.1
  169.6 31.9 %reduce-scatter.3.cloned.1.call-done = bf16[96,2048]{1,0:T(8,128)(2,1)} async-done(((bf16[384,2048]{1,0:T(8,128)(2,1)}), bf16[96,2048]{1,0:T(8,128)(2,1)}) %reduce-scatter.3.cloned.1.call-update) | async-done | bytes 393232 | tf_op jit(solution)/shard_map/reduce_scatter | solution.py:224
  201.5 1.2 multiply_reduce_fusion
  202.8 1.9 multiply_convert_fusion
  206.8 17.7 %all-gather.5.cloned.1.call-done = bf16[384,2048]{1,0:T(8,128)(2,1)} async-done(((bf16[96,2048]{1,0:T(8,128)(2,1)}), bf16[384,2048]{1,0:T(8,128)(2,1)}) %all-gather.5.cloned.1.call-update) | async-done | bytes 1572880 | tf_op jit(solution)/shard_map/all_gather | solution.py:232
  224.5 94.5 %all-gather.7.cloned.1.call-done = bf16[2048,1408]{1,0:T(8,128)(2,1)} async-done(((bf16[256,1408]{1,0:T(8,128)(2,1)}), bf16[2048,1408]{1,0:T(8,128)(2,1)}) %all-gather.7.cloned.1.call-update) | async-done | bytes 5767184 | tf_op jit(solution)/shard_map/all_gather | solution.py:170
  319.0 7.1 %fusion.84 = f32[384,1408]{1,0:T(8,128)} fusion(bf16[384,2048]{1,0:T(8,128)(2,1)} %all-gather.5.cloned.1.call-done, bf16[2048,1408]{1,0:T(8,128)(2,1)} %all-gather.7.cloned.1.call-done), kind=kOutput, calls=%fused_computation.133 | convolution fusion | flops 2214592512 | bytes 9502720 | tf_op jit(solution)/shard_map/dot_general | solution.py:173
  326.1 86.2 %all-gather.11.cloned.1.call-done = bf16[1408,2048]{1,0:T(8,128)(2,1)} async-done(((bf16[1408,256]{1,0:T(8,128)(2,1)}), bf16[1408,2048]{1,0:T(8,128)(2,1)}) %all-gather.11.cloned.1.call-update) | async-done | bytes 5767184 | tf_op jit(solution)/shard_map/all_gather | solution.py:176
  412.3 92.6 %all-gather.9.cloned.1.call-done = bf16[2048,1408]{1,0:T(8,128)(2,1)} async-done(((bf16[256,1408]{1,0:T(8,128)(2,1)}), bf16[2048,1408]{1,0:T(8,128)(2,1)}) %all-gather.9.cloned.1.call-update) | async-done | bytes 5767184 | tf_op jit(solution)/shard_map/all_gather | solution.py:171
  504.8 11.3 %convolution_convert_fusion = bf16[384,2048]{1,0:T(8,128)(2,1)} fusion(bf16[1408,2048]{1,0:T(8,128)(2,1)} %all-gather.11.cloned.1.call-done, bf16[384,2048]{1,0:T(8,128)(2,1)S(1)} %copy-done.7, bf16[2048,1408]{1,0:T(8,128)(2,1)} %all-gather.9.cloned.1.call-done, f32[384,1408]{1,0:T(8,128)} %fusion.84), kind=kOutput, calls=%fused_computation.52 | convolution fusion | flops 4433215488 | bytes 16842752 | tf_op jit(solution)/shard_map/dot_general | solution.py:177
  516.1 26.4 %reduce-scatter.5.cloned.1.call-done = bf16[96,2048]{1,0:T(8,128)(2,1)} async-done(((bf16[384,2048]{1,0:T(8,128)(2,1)}), bf16[96,2048]{1,0:T(8,128)(2,1)}) %reduce-scatter.5.cloned.1.call-update) | async-done | bytes 393232 | tf_op jit(solution)/shard_map/reduce_scatter | solution.py:234
  542.5 1.9 add_convert_fusion
  (105 shorter events, 19.7 us)
Async XLA Ops:
  6.5 161.2 %copy-start = (bf16[256,2048]{1,0:T(8,128)(2,1)S(1)}, bf16[256,2048]{1,0:T(8,128)(2,1)}, u32[]{:S(2)}) copy-start(bf16[256,2048]{1,0:T(8,128)(2,1)} %param.29) | copy-start | bytes 3145732
  6.5 195.0 %reduce-scatter.3.cloned.1.call-start = ((), (), s32[]{:S(2)}) async-start(), calls=%async_computation.2 | async-start | bytes 1966080 | tf_op jit(solution)/shard_map/reduce_scatter | solution.py:224
  75.6 1.1 copy-start.4
  115.7 51.0 %copy-start.3 = (f32[6,2,64,128]{3,2,0,1:T(8,128)S(1)}, f32[6,2,64,128]{3,2,0,1:T(8,128)}, u32[]{:S(2)}) copy-start(f32[6,2,64,128]{3,2,0,1:T(8,128)} %get-tuple-element.93) | copy-start | bytes 1179652
  116.9 50.5 %copy-start.6 = (f32[128]{0:T(128)S(1)}, f32[128]{0:T(128)}, u32[]{:S(2)}) copy-start(f32[128]{0:T(128)} %param.28) | copy-start | bytes 1540
  117.2 6.8 %collective-permute-start = (bf16[2,128,128]{2,1,0:T(8,128)(2,1)S(1)}, bf16[2,128,128]{2,1,0:T(8,128)(2,1)S(1)}, u32[]{:S(2)}, u32[]{:S(2)}) collective-permute-start(bf16[2,128,128]{2,1,0:T(8,128)(2,1)S(1)} %fusion.150), channel_id=1, source_target_pairs={{0,4},{4,8},{8,12},{12,16},{16,20},{20,24},{24,28},{1,5},{5,9},{9,... | collective-permute-start | bytes 196616 | tf_op jit(solution)/shard_map/while/body/eval_jaxpr/ppermute | solution.py:15
  124.3 6.2 %collective-permute-start = (bf16[2,128,128]{2,1,0:T(8,128)(2,1)S(1)}, bf16[2,128,128]{2,1,0:T(8,128)(2,1)S(1)}, u32[]{:S(2)}, u32[]{:S(2)}) collective-permute-start(bf16[2,128,128]{2,1,0:T(8,128)(2,1)S(1)} %fusion.150), channel_id=1, source_target_pairs={{0,4},{4,8},{8,12},{12,16},{16,20},{20,24},{24,28},{1,5},{5,9},{9,... | collective-permute-start | bytes 196616 | tf_op jit(solution)/shard_map/while/body/eval_jaxpr/ppermute | solution.py:15
  130.8 6.2 %collective-permute-start = (bf16[2,128,128]{2,1,0:T(8,128)(2,1)S(1)}, bf16[2,128,128]{2,1,0:T(8,128)(2,1)S(1)}, u32[]{:S(2)}, u32[]{:S(2)}) collective-permute-start(bf16[2,128,128]{2,1,0:T(8,128)(2,1)S(1)} %fusion.150), channel_id=1, source_target_pairs={{0,4},{4,8},{8,12},{12,16},{16,20},{20,24},{24,28},{1,5},{5,9},{9,... | collective-permute-start | bytes 196616 | tf_op jit(solution)/shard_map/while/body/eval_jaxpr/ppermute | solution.py:15
  137.3 7.1 %collective-permute-start = (bf16[2,128,128]{2,1,0:T(8,128)(2,1)S(1)}, bf16[2,128,128]{2,1,0:T(8,128)(2,1)S(1)}, u32[]{:S(2)}, u32[]{:S(2)}) collective-permute-start(bf16[2,128,128]{2,1,0:T(8,128)(2,1)S(1)} %fusion.150), channel_id=1, source_target_pairs={{0,4},{4,8},{8,12},{12,16},{16,20},{20,24},{24,28},{1,5},{5,9},{9,... | collective-permute-start | bytes 196616 | tf_op jit(solution)/shard_map/while/body/eval_jaxpr/ppermute | solution.py:15
  144.7 7.1 %collective-permute-start = (bf16[2,128,128]{2,1,0:T(8,128)(2,1)S(1)}, bf16[2,128,128]{2,1,0:T(8,128)(2,1)S(1)}, u32[]{:S(2)}, u32[]{:S(2)}) collective-permute-start(bf16[2,128,128]{2,1,0:T(8,128)(2,1)S(1)} %fusion.150), channel_id=1, source_target_pairs={{0,4},{4,8},{8,12},{12,16},{16,20},{20,24},{24,28},{1,5},{5,9},{9,... | collective-permute-start | bytes 196616 | tf_op jit(solution)/shard_map/while/body/eval_jaxpr/ppermute | solution.py:15
  152.1 7.4 %collective-permute-start = (bf16[2,128,128]{2,1,0:T(8,128)(2,1)S(1)}, bf16[2,128,128]{2,1,0:T(8,128)(2,1)S(1)}, u32[]{:S(2)}, u32[]{:S(2)}) collective-permute-start(bf16[2,128,128]{2,1,0:T(8,128)(2,1)S(1)} %fusion.150), channel_id=1, source_target_pairs={{0,4},{4,8},{8,12},{12,16},{16,20},{20,24},{24,28},{1,5},{5,9},{9,... | collective-permute-start | bytes 196616 | tf_op jit(solution)/shard_map/while/body/eval_jaxpr/ppermute | solution.py:15
  159.7 7.0 %collective-permute-start = (bf16[2,128,128]{2,1,0:T(8,128)(2,1)S(1)}, bf16[2,128,128]{2,1,0:T(8,128)(2,1)S(1)}, u32[]{:S(2)}, u32[]{:S(2)}) collective-permute-start(bf16[2,128,128]{2,1,0:T(8,128)(2,1)S(1)} %fusion.150), channel_id=1, source_target_pairs={{0,4},{4,8},{8,12},{12,16},{16,20},{20,24},{24,28},{1,5},{5,9},{9,... | collective-permute-start | bytes 196616 | tf_op jit(solution)/shard_map/while/body/eval_jaxpr/ppermute | solution.py:15
  166.7 1.0 copy-start.8
  167.7 33.8 %copy-start.1 = (bf16[96,2048]{1,0:T(8,128)(2,1)S(1)}, bf16[96,2048]{1,0:T(8,128)(2,1)}, u32[]{:S(2)}) copy-start(bf16[96,2048]{1,0:T(8,128)(2,1)} %param.19) | copy-start | bytes 1179652
  167.7 35.0 %copy-start.5 = (f32[2048]{0:T(1024)S(1)}, f32[2048]{0:T(1024)}, u32[]{:S(2)}) copy-start(f32[2048]{0:T(1024)} %param.30) | copy-start | bytes 24580
  169.6 54.9 %all-gather.5.cloned.1.call-start = ((), (), s32[]{:S(2)}) async-start(), calls=%async_computation.3 | async-start | bytes 1966080 | tf_op jit(solution)/shard_map/all_gather | solution.py:232
  204.7 114.3 %all-gather.7.cloned.1.call-start = ((), (), s32[]{:S(2)}) async-start(), calls=%async_computation.4 | async-start | bytes 6488064 | tf_op jit(solution)/shard_map/all_gather | solution.py:170
  205.4 206.8 %all-gather.11.cloned.1.call-start = ((), (), s32[]{:S(2)}) async-start(), calls=%async_computation.6 | async-start | bytes 6488064 | tf_op jit(solution)/shard_map/all_gather | solution.py:176
  206.0 298.8 %all-gather.9.cloned.1.call-start = ((), (), s32[]{:S(2)}) async-start(), calls=%async_computation.5 | async-start | bytes 6488064 | tf_op jit(solution)/shard_map/all_gather | solution.py:171
  206.6 335.9 %reduce-scatter.5.cloned.1.call-start = ((), (), s32[]{:S(2)}) async-start(), calls=%async_computation.7 | async-start | bytes 1966080 | tf_op jit(solution)/shard_map/reduce_scatter | solution.py:234
  224.5 280.3 %copy-start.7 = (bf16[384,2048]{1,0:T(8,128)(2,1)S(1)}, bf16[384,2048]{1,0:T(8,128)(2,1)}, u32[]{:S(2)}) copy-start(bf16[384,2048]{1,0:T(8,128)(2,1)} %all-gather.5.cloned.1.call-done) | copy-start | bytes 4718596
  326.1 216.4 %copy-start.2 = (bf16[96,2048]{1,0:T(8,128)(2,1)S(1)}, bf16[96,2048]{1,0:T(8,128)(2,1)}, u32[]{:S(2)}) copy-start(bf16[96,2048]{1,0:T(8,128)(2,1)} %reduce-scatter.3.cloned.1.call-done) | copy-start | bytes 1179652
Sparse Core Ops, SparseCore 0:
  169.7 31.7 reduce-scatter.2
  204.8 19.6 all-gather.4
  226.7 92.3 all-gather.6
  320.9 91.2 all-gather.10
  414.3 90.4 all-gather.8
  516.2 26.1 reduce-scatter.4
where the time goes:
time: 553 us; the launch traced here: 551 us
  waiting for transfers between devices  364 us (66%)
  other arithmetic  74.1 us (13%)
  matrix products  60.9 us (11%)
  starting transfers between devices  34.5 us (6%)
  between operations  13.7 us (2%)
    all_gather x1, waiting for transfers between devices, feed_forward(): lax.all_gather(gate_matrix, 'sp', axis=0, tiled=True)  94.5 us
    all_gather x1, waiting for transfers between devices, feed_forward(): lax.all_gather(up_matrix, 'sp', axis=0, tiled=True)  92.6 us
    all_gather x1, waiting for transfers between devices, feed_forward(): down_whole = lax.all_gather(down_matrix, 'sp', axis=1, tiled=True)  86.2 us
    another operation x2, other arithmetic, block_correction(): lax.linalg.triangular_solve(system, right_side, left_side=True, lower=Tru...  59.6 us
    ppermute x7, starting transfers between devices, from_behind(): return lax.ppermute(value, axis, pairs)  34.2 us
    reduce_scatter x1, waiting for transfers between devices, body(): lax.psum_scatter(jnp.dot(mixed, head_output_matrix, preferred_element_typ...  31.9 us
    reduce_scatter x1, waiting for transfers between devices, body(): lax.psum_scatter(ffn_term.astype(jnp.bfloat16), 'tp', scatter_dimension=0...  26.4 us
    all_gather x1, waiting for transfers between devices, body(): whole_rows = lax.all_gather(normed_own, 'tp', axis=0, tiled=True)  17.7 us
  transfers between devices with their start and end apart: 13, of which 13 were waited for; matrix products, arithmetic and copies ran while one was open for 1% of the time, Pallas kernels for 0%

commit v1 on v0

--- a/solution.py
+++ b/solution.py
@@ -173,7 +173,12 @@
     gate_total = jnp.dot(whole_rows, gate_whole, preferred_element_type=jnp.float32)
     up_total = jnp.dot(whole_rows, up_whole, preferred_element_type=jnp.float32)
     hidden = (jax.nn.silu(gate_total) * up_total).astype(jnp.bfloat16)
-    down_whole = lax.all_gather(down_matrix, "sp", axis=1, tiled=True)
+    ring = [down_matrix]
+    for hop in range(7):
+        ring.append(lax.ppermute(ring[-1], "sp", [(dev, (dev + 1) % 8) for dev in range(8)]))
+    down_whole = jnp.roll(
+        jnp.concatenate(ring[::-1], axis=1), (lax.axis_index("sp") + 1) * ring[0].shape[1], axis=1
+    )
     return jnp.dot(hidden, down_whole, preferred_element_type=jnp.float32)
 
 

time: 553 us -> 534 us (0.966)
  waiting for transfers between devices: 364 us -> 307 us
  local copies, waits for them, and re-layouts: 2.78 us -> 31 us
  matrix products: 60.9 us -> 70.4 us
    ppermute x0 -> x7, waiting for transfers between devices: none -> 202 us  [feed_forward(): lax.ppermute(ring[-1], 'sp', [(dev, (dev + 1) % 8) for dev in range(8)])]
    all_gather x1, waiting for transfers between devices: 94.5 us -> 0.01 us  [feed_forward(): lax.all_gather(gate_matrix, 'sp', axis=0, tiled=True)]
    all_gather x1 -> x0, waiting for transfers between devices: 86.2 us -> none  [feed_forward(): down_whole = lax.all_gather(down_matrix, 'sp', axis=1, tiled=True)]
    all_gather x1, waiting for transfers between devices: 92.6 us -> 31.6 us  [feed_forward(): lax.all_gather(up_matrix, 'sp', axis=0, tiled=True)]
    unnamed x19 -> x44, local copies, waits for them, and re-layouts: 0.17 us -> 27.5 us
    all_gather x1, waiting for transfers between devices: 17.7 us -> 0.01 us  [body(): whole_rows = lax.all_gather(normed_own, 'tp', axis=0, tiled=True)]
  transfers between devices with their start and end apart: 13 -> 19, of which waited for: 13 -> 17; matrix products, arithmetic and copies ran while one was open for 1% -> 6% of each run, Pallas kernels for 0% -> 0%
where the time goes in v1:
time: 534 us; the launch traced here: 532 us
  waiting for transfers between devices  307 us (57%)
  other arithmetic  74.1 us (14%)
  matrix products  70.4 us (13%)
  starting transfers between devices  35.9 us (7%)
  local copies, waits for them, and re-layouts  31 us (6%)
  between operations  13.4 us (3%)
    ppermute x7, waiting for transfers between devices, feed_forward(): lax.ppermute(ring[-1], 'sp', [(dev, (dev + 1) % 8) for dev in range(8)])  202 us
    another operation x2, other arithmetic, block_correction(): lax.linalg.triangular_solve(system, right_side, left_side=True, lower=Tru...  59.6 us
    ppermute x7, starting transfers between devices, from_behind(): return lax.ppermute(value, axis, pairs)  34.2 us
    reduce_scatter x1, waiting for transfers between devices, body(): lax.psum_scatter(jnp.dot(mixed, head_output_matrix, preferred_element_typ...  31.9 us
    all_gather x1, waiting for transfers between devices, feed_forward(): lax.all_gather(up_matrix, 'sp', axis=0, tiled=True)  31.6 us
    unnamed x44, local copies, waits for them, and re-layouts  27.5 us
    reduce_scatter x1, waiting for transfers between devices, body(): lax.psum_scatter(ffn_term.astype(jnp.bfloat16), 'tp', scatter_dimension=0...  26.4 us
    ppermute x7, waiting for transfers between devices, from_behind(): return lax.ppermute(value, axis, pairs)  13.4 us
  transfers between devices with their start and end apart: 19, of which 17 were waited for; matrix products, arithmetic and copies ran while one was open for 6% of the time, Pallas kernels for 0%

profile of v1, /device:TPU:0, one launch (start us, length us, event | category | flops | bytes accessed | tf_op | source)
XLA Modules:
  0.0 532.2 jit_solution(2902205664689989090)
XLA Ops:
  8.9 1.1 fusion.69
  10.0 1.1 fusion.67
  12.0 1.1 fusion.65
  13.1 1.1 fusion.66
  16.1 59.6 %custom-call.3 = f32[2,6,1,64,64]{3,4,2,1,0:T(8,128)} custom-call(f32[2,6,1,64,64]{4,3,2,1,0:T(8,128)S(1)} %fusion.53), custom_call_target="InvertDiagBlocksLowerTriangular" | custom-call | tf_op jit(solution)/shard_map/triangular_solve | solution.py:63
  75.7 1.1 multiply_multiply_fusion
  76.8 1.8 fusion.54
  79.5 1.5 fusion.49
  81.1 41.8 %while.28 = (s32[]{:T(128)}, f32[2,128,128]{2,1,0:T(8,128)S(1)}, f32[2,128,128]{2,1,0:T(8,128)S(1)}, f32[6,2,64,128]{3,2,0,1:T(8,128)}, f32[6,2,64,128]{3,2,0,1:...) while((s32[]{:T(128)}, f32[2,128,128]{2,1,0:T(8,128)S(1)}, ...), condition=%wide.region_4.5_spmd.clone, body=%wide.region_3.4_spmd.clone.sunk | while | flops 201605120 | bytes 2758840 | solution.py:152
  81.1 1.2 fusion.150
  82.3 1.1 convolution_subtract_fusion.6
  86.5 1.7 fusion.151
  89.2 1.1 convolution_subtract_fusion.6
  93.4 1.7 fusion.151
  96.2 1.1 convolution_subtract_fusion.6
  100.4 1.7 fusion.151
  103.1 1.1 convolution_subtract_fusion.6
  107.3 1.7 fusion.151
  110.1 1.1 convolution_subtract_fusion.6
  114.2 1.7 fusion.151
  117.0 1.1 convolution_subtract_fusion.6
  121.2 1.7 fusion.151
  122.9 1.2 copy.42
  124.0 49.8 %while.29 = (s32[]{:T(128)}, f32[2,128,128]{2,1,0:T(8,128)S(1)}, f32[2,128,128]{2,1,0:T(8,128)S(1)}, f32[2,128,128]{2,1,0:T(8,128)S(1)}, s32[]{:T(128)}, /*index=5*/s32[]{:T(128)}) while((s32[]{:T(128)}, f32[2,128,128]{2,1,0:T(8,128)S(1)}, f32[2,128,128]{2,1,0:T(8,128)S(1)}, f32[2,128,128]{2,1,0:T(8,128)S(1)}, s32[]{:T(128)}, ...), condition=%wide.region_6.7_spmd.clone, body=%wide.region_5.6_spmd.clone.sunk | while | flops 50462720 | bytes 917623 | solution.py:220
  124.3 4.9 collective-permute-start
  129.2 1.9 collective-permute-done
  131.4 4.3 collective-permute-start
  135.7 1.9 collective-permute-done
  137.9 4.3 collective-permute-start
  142.2 1.9 collective-permute-done
  144.4 5.2 collective-permute-start
  149.6 1.9 collective-permute-done
  151.8 5.2 collective-permute-start
  157.0 1.9 collective-permute-done
  159.1 5.3 collective-permute-start
  164.4 2.1 collective-permute-done
  166.8 5.1 collective-permute-start
  171.9 1.9 collective-permute-done
  173.8 1.7 multiply_reduce_fusion.1
  175.8 2.7 convolution_convert_fusion
  178.6 31.9 %reduce-scatter.3.cloned.1.call-done = bf16[96,2048]{1,0:T(8,128)(2,1)} async-done(((bf16[384,2048]{1,0:T(8,128)(2,1)}), bf16[96,2048]{1,0:T(8,128)(2,1)}) %reduce-scatter.3.cloned.1.call-update) | async-done | bytes 393232 | tf_op jit(solution)/shard_map/reduce_scatter | solution.py:229
  210.4 1.2 multiply_reduce_fusion
  211.7 1.9 multiply_convert_fusion
  215.0 1.5 collective-permute-start.1
  216.5 18.9 %collective-permute-done.1 = bf16[1408,256]{1,0:T(8,128)(2,1)S(1)} collective-permute-done((bf16[1408,256]{1,0:T(8,128)(2,1)S(1)}, bf16[1408,256]{1,0:T(8,128)(2,1)S(1)}, u32[]{:S(2)}, u32[]{:S(2)}) %collective-permute-start.1) | collective-permute-done | bytes 720928 | tf_op jit(solution)/shard_map/ppermute | solution.py:178
  235.5 27.2 %collective-permute-done.2 = bf16[1408,256]{1,0:T(8,128)(2,1)S(1)} collective-permute-done((bf16[1408,256]{1,0:T(8,128)(2,1)S(1)}, bf16[1408,256]{1,0:T(8,128)(2,1)S(1)}, u32[]{:S(2)}, u32[]{:S(2)}) %collective-permute-start.2) | collective-permute-done | bytes 720928 | tf_op jit(solution)/shard_map/ppermute | solution.py:178
  263.5 30.2 %collective-permute-done.3 = bf16[1408,256]{1,0:T(8,128)(2,1)S(1)} collective-permute-done((bf16[1408,256]{1,0:T(8,128)(2,1)S(1)}, bf16[1408,256]{1,0:T(8,128)(2,1)S(1)}, u32[]{:S(2)}, u32[]{:S(2)}) %collective-permute-start.3) | collective-permute-done | bytes 720928 | tf_op jit(solution)/shard_map/ppermute | solution.py:178
  294.6 35.0 %collective-permute-done.4 = bf16[1408,256]{1,0:T(8,128)(2,1)S(1)} collective-permute-done((bf16[1408,256]{1,0:T(8,128)(2,1)S(1)}, bf16[1408,256]{1,0:T(8,128)(2,1)S(1)}, u32[]{:S(2)}, u32[]{:S(2)}) %collective-permute-start.4) | collective-permute-done | bytes 720928 | tf_op jit(solution)/shard_map/ppermute | solution.py:178
  330.5 35.1 %collective-permute-done.5 = bf16[1408,256]{1,0:T(8,128)(2,1)S(1)} collective-permute-done((bf16[1408,256]{1,0:T(8,128)(2,1)S(1)}, bf16[1408,256]{1,0:T(8,128)(2,1)S(1)}, u32[]{:S(2)}, u32[]{:S(2)}) %collective-permute-start.5) | collective-permute-done | bytes 720928 | tf_op jit(solution)/shard_map/ppermute | solution.py:178
  366.5 23.5 %collective-permute-done.6 = bf16[1408,256]{1,0:T(8,128)(2,1)} collective-permute-done((bf16[1408,256]{1,0:T(8,128)(2,1)S(1)}, bf16[1408,256]{1,0:T(8,128)(2,1)}, u32[]{:S(2)}, u32[]{:S(2)}) %collective-permute-start.6) | collective-permute-done | bytes 720928 | tf_op jit(solution)/shard_map/ppermute | solution.py:178
  390.1 32.3 %collective-permute-done.7 = bf16[1408,256]{1,0:T(8,128)(2,1)} collective-permute-done((bf16[1408,256]{1,0:T(8,128)(2,1)}, bf16[1408,256]{1,0:T(8,128)(2,1)}, u32[]{:S(2)}, u32[]{:S(2)}) %collective-permute-start.7) | collective-permute-done | bytes 720928 | tf_op jit(solution)/shard_map/ppermute | solution.py:178
  422.4 2.1 constant_dynamic-update-slice_fusion.15
  424.4 2.1 constant_dynamic-update-slice_fusion.14
  426.5 2.1 constant_dynamic-update-slice_fusion.13
  428.6 2.1 constant_dynamic-update-slice_fusion.12
  430.7 2.1 constant_dynamic-update-slice_fusion.11
  432.8 2.3 constant_dynamic-update-slice_fusion.10
  437.1 2.1 constant_dynamic-update-slice_fusion.7
  439.1 2.1 constant_dynamic-update-slice_fusion.6
  447.0 7.1 %fusion.90 = f32[384,1408]{1,0:T(8,128)} fusion(bf16[384,2048]{1,0:T(8,128)(2,1)} %all-gather.4.cloned.1.call-done, bf16[2048,1408]{1,0:T(8,128)(2,1)} %all-gather.6.cloned.1.call-done), kind=kOutput, calls=%fused_computation.152 | convolution fusion | flops 2214592512 | bytes 9502720 | tf_op jit(solution)/shard_map/dot_general | solution.py:173
  454.1 31.6 %all-gather.8.cloned.1.call-done = bf16[2048,1408]{1,0:T(8,128)(2,1)} async-done(((bf16[256,1408]{1,0:T(8,128)(2,1)}), bf16[2048,1408]{1,0:T(8,128)(2,1)}) %all-gather.8.cloned.1.call-update) | async-done | bytes 5767184 | tf_op jit(solution)/shard_map/all_gather | solution.py:171
  485.7 11.7 %fusion.46 = bf16[384,2048]{1,0:T(8,128)(2,1)} fusion(bf16[1408,4096]{1,0:T(8,128)(2,1)} %constant_dynamic-update-slice_fusion, s32[]{:T(128)S(6)} %select_n.44, bf16[384,2048]{1,0:T(8,128)(2,1)} %all-gather.4.cloned.1.call-done, bf16[2048,1408]{1,0:T(8,128)(2,1)} %all-gather.8.cloned.1.call-done, f32[384,1408]{1,0:T(8,128)} %fusion.90), kind=kOutput, calls=%fused_computation.54 | convolution fusion | flops 4433215488 | bytes 16842756 | tf_op jit(solution)/shard_map/dot_general | solution.py:182
  497.4 26.4 %reduce-scatter.5.cloned.1.call-done = bf16[96,2048]{1,0:T(8,128)(2,1)} async-done(((bf16[384,2048]{1,0:T(8,128)(2,1)}), bf16[96,2048]{1,0:T(8,128)(2,1)}) %reduce-scatter.5.cloned.1.call-update) | async-done | bytes 393232 | tf_op jit(solution)/shard_map/reduce_scatter | solution.py:239
  523.7 1.9 add_convert_fusion
  (142 shorter events, 44.5 us)
Async XLA Ops:
  6.5 169.2 %copy-start = (bf16[256,2048]{1,0:T(8,128)(2,1)S(1)}, bf16[256,2048]{1,0:T(8,128)(2,1)}, u32[]{:S(2)}) copy-start(bf16[256,2048]{1,0:T(8,128)(2,1)} %param.29) | copy-start | bytes 3145732
  6.5 203.9 %reduce-scatter.3.cloned.1.call-start = ((), (), s32[]{:S(2)}) async-start(), calls=%async_computation.2 | async-start | bytes 1966080 | tf_op jit(solution)/shard_map/reduce_scatter | solution.py:229
  78.7 96.8 %copy-start.13 = (f32[128]{0:T(128)S(1)}, f32[128]{0:T(128)}, u32[]{:S(2)}) copy-start(f32[128]{0:T(128)} %param.28) | copy-start | bytes 1540
  81.1 129.4 %copy-start.1 = (bf16[96,2048]{1,0:T(8,128)(2,1)S(1)}, bf16[96,2048]{1,0:T(8,128)(2,1)}, u32[]{:S(2)}) copy-start(bf16[96,2048]{1,0:T(8,128)(2,1)} %param.19) | copy-start | bytes 1179652
  81.1 130.6 %copy-start.12 = (f32[2048]{0:T(1024)S(1)}, f32[2048]{0:T(1024)}, u32[]{:S(2)}) copy-start(f32[2048]{0:T(1024)} %param.30) | copy-start | bytes 24580
  81.1 133.9 %copy-start.3 = (bf16[1408,256]{1,0:T(8,128)(2,1)S(1)}, bf16[1408,256]{1,0:T(8,128)(2,1)}, u32[]{:S(2)}) copy-start(bf16[1408,256]{1,0:T(8,128)(2,1)} %param.33) | copy-start | bytes 2162692
  124.3 6.8 %collective-permute-start = (bf16[2,128,128]{2,1,0:T(8,128)(2,1)S(1)}, bf16[2,128,128]{2,1,0:T(8,128)(2,1)S(1)}, u32[]{:S(2)}, u32[]{:S(2)}) collective-permute-start(bf16[2,128,128]{2,1,0:T(8,128)(2,1)S(1)} %fusion.155), channel_id=1, source_target_pairs={{0,4},{4,8},{8,12},{12,16},{16,20},{20,24},{24,28},{1,5},{5,9},{9,... | collective-permute-start | bytes 196616 | tf_op jit(solution)/shard_map/while/body/eval_jaxpr/ppermute | solution.py:15
  131.4 6.2 %collective-permute-start = (bf16[2,128,128]{2,1,0:T(8,128)(2,1)S(1)}, bf16[2,128,128]{2,1,0:T(8,128)(2,1)S(1)}, u32[]{:S(2)}, u32[]{:S(2)}) collective-permute-start(bf16[2,128,128]{2,1,0:T(8,128)(2,1)S(1)} %fusion.155), channel_id=1, source_target_pairs={{0,4},{4,8},{8,12},{12,16},{16,20},{20,24},{24,28},{1,5},{5,9},{9,... | collective-permute-start | bytes 196616 | tf_op jit(solution)/shard_map/while/body/eval_jaxpr/ppermute | solution.py:15
  137.9 6.2 %collective-permute-start = (bf16[2,128,128]{2,1,0:T(8,128)(2,1)S(1)}, bf16[2,128,128]{2,1,0:T(8,128)(2,1)S(1)}, u32[]{:S(2)}, u32[]{:S(2)}) collective-permute-start(bf16[2,128,128]{2,1,0:T(8,128)(2,1)S(1)} %fusion.155), channel_id=1, source_target_pairs={{0,4},{4,8},{8,12},{12,16},{16,20},{20,24},{24,28},{1,5},{5,9},{9,... | collective-permute-start | bytes 196616 | tf_op jit(solution)/shard_map/while/body/eval_jaxpr/ppermute | solution.py:15
  144.4 7.1 %collective-permute-start = (bf16[2,128,128]{2,1,0:T(8,128)(2,1)S(1)}, bf16[2,128,128]{2,1,0:T(8,128)(2,1)S(1)}, u32[]{:S(2)}, u32[]{:S(2)}) collective-permute-start(bf16[2,128,128]{2,1,0:T(8,128)(2,1)S(1)} %fusion.155), channel_id=1, source_target_pairs={{0,4},{4,8},{8,12},{12,16},{16,20},{20,24},{24,28},{1,5},{5,9},{9,... | collective-permute-start | bytes 196616 | tf_op jit(solution)/shard_map/while/body/eval_jaxpr/ppermute | solution.py:15
  151.8 7.1 %collective-permute-start = (bf16[2,128,128]{2,1,0:T(8,128)(2,1)S(1)}, bf16[2,128,128]{2,1,0:T(8,128)(2,1)S(1)}, u32[]{:S(2)}, u32[]{:S(2)}) collective-permute-start(bf16[2,128,128]{2,1,0:T(8,128)(2,1)S(1)} %fusion.155), channel_id=1, source_target_pairs={{0,4},{4,8},{8,12},{12,16},{16,20},{20,24},{24,28},{1,5},{5,9},{9,... | collective-permute-start | bytes 196616 | tf_op jit(solution)/shard_map/while/body/eval_jaxpr/ppermute | solution.py:15
  159.1 7.4 %collective-permute-start = (bf16[2,128,128]{2,1,0:T(8,128)(2,1)S(1)}, bf16[2,128,128]{2,1,0:T(8,128)(2,1)S(1)}, u32[]{:S(2)}, u32[]{:S(2)}) collective-permute-start(bf16[2,128,128]{2,1,0:T(8,128)(2,1)S(1)} %fusion.155), channel_id=1, source_target_pairs={{0,4},{4,8},{8,12},{12,16},{16,20},{20,24},{24,28},{1,5},{5,9},{9,... | collective-permute-start | bytes 196616 | tf_op jit(solution)/shard_map/while/body/eval_jaxpr/ppermute | solution.py:15
  166.8 7.0 %collective-permute-start = (bf16[2,128,128]{2,1,0:T(8,128)(2,1)S(1)}, bf16[2,128,128]{2,1,0:T(8,128)(2,1)S(1)}, u32[]{:S(2)}, u32[]{:S(2)}) collective-permute-start(bf16[2,128,128]{2,1,0:T(8,128)(2,1)S(1)} %fusion.155), channel_id=1, source_target_pairs={{0,4},{4,8},{8,12},{12,16},{16,20},{20,24},{24,28},{1,5},{5,9},{9,... | collective-permute-start | bytes 196616 | tf_op jit(solution)/shard_map/while/body/eval_jaxpr/ppermute | solution.py:15
  178.5 268.5 %all-gather.4.cloned.1.call-start = ((), (), s32[]{:S(2)}) async-start(), calls=%async_computation.3 | async-start | bytes 1966080 | tf_op jit(solution)/shard_map/all_gather | solution.py:237
  213.6 233.4 %all-gather.6.cloned.1.call-start = ((), (), s32[]{:S(2)}) async-start(), calls=%async_computation.4 | async-start | bytes 6488064 | tf_op jit(solution)/shard_map/all_gather | solution.py:170
  214.4 271.3 %all-gather.8.cloned.1.call-start = ((), (), s32[]{:S(2)}) async-start(), calls=%async_computation.5 | async-start | bytes 6488064 | tf_op jit(solution)/shard_map/all_gather | solution.py:171
  214.9 308.8 %reduce-scatter.5.cloned.1.call-start = ((), (), s32[]{:S(2)}) async-start(), calls=%async_computation.6 | async-start | bytes 1966080 | tf_op jit(solution)/shard_map/reduce_scatter | solution.py:239
  215.0 20.5 %collective-permute-start.1 = (bf16[1408,256]{1,0:T(8,128)(2,1)S(1)}, bf16[1408,256]{1,0:T(8,128)(2,1)S(1)}, u32[]{:S(2)}, u32[]{:S(2)}) collective-permute-start(bf16[1408,256]{1,0:T(8,128)(2,1)S(1)} %copy-done.3), channel_id=1, source_target_pairs={{0,4},{4,8},{8,12},{12,16},{16,20},{20,24},{24,28},{28,0},{1,5},{5... | collective-permute-start | bytes 2162696 | tf_op jit(solution)/shard_map/ppermute | solution.py:178
  235.5 27.2 %collective-permute-start.2 = (bf16[1408,256]{1,0:T(8,128)(2,1)S(1)}, bf16[1408,256]{1,0:T(8,128)(2,1)S(1)}, u32[]{:S(2)}, u32[]{:S(2)}) collective-permute-start(bf16[1408,256]{1,0:T(8,128)(2,1)S(1)} %collective-permute-done.1), channel_id=1, source_target_pairs={{0,4},{4,8},{8,12},{12,16},{16,20},{20,24},{24,28},{28,0},{1,5},{5... | collective-permute-start | bytes 2162696 | tf_op jit(solution)/shard_map/ppermute | solution.py:178
  262.6 0.9 copy-start.4
  263.5 30.2 %collective-permute-start.3 = (bf16[1408,256]{1,0:T(8,128)(2,1)S(1)}, bf16[1408,256]{1,0:T(8,128)(2,1)S(1)}, u32[]{:S(2)}, u32[]{:S(2)}) collective-permute-start(bf16[1408,256]{1,0:T(8,128)(2,1)S(1)} %collective-permute-done.2), channel_id=1, source_target_pairs={{0,4},{4,8},{8,12},{12,16},{16,20},{20,24},{24,28},{28,0},{1,5},{5... | collective-permute-start | bytes 2162696 | tf_op jit(solution)/shard_map/ppermute | solution.py:178
  293.7 0.9 copy-start.6
  294.6 35.0 %collective-permute-start.4 = (bf16[1408,256]{1,0:T(8,128)(2,1)S(1)}, bf16[1408,256]{1,0:T(8,128)(2,1)S(1)}, u32[]{:S(2)}, u32[]{:S(2)}) collective-permute-start(bf16[1408,256]{1,0:T(8,128)(2,1)S(1)} %collective-permute-done.3), channel_id=1, source_target_pairs={{0,4},{4,8},{8,12},{12,16},{16,20},{20,24},{24,28},{28,0},{1,5},{5... | collective-permute-start | bytes 2162696 | tf_op jit(solution)/shard_map/ppermute | solution.py:178
  329.6 0.9 copy-start.8
  330.5 35.1 %collective-permute-start.5 = (bf16[1408,256]{1,0:T(8,128)(2,1)S(1)}, bf16[1408,256]{1,0:T(8,128)(2,1)S(1)}, u32[]{:S(2)}, u32[]{:S(2)}) collective-permute-start(bf16[1408,256]{1,0:T(8,128)(2,1)S(1)} %collective-permute-done.4), channel_id=1, source_target_pairs={{0,4},{4,8},{8,12},{12,16},{16,20},{20,24},{24,28},{28,0},{1,5},{5... | collective-permute-start | bytes 2162696 | tf_op jit(solution)/shard_map/ppermute | solution.py:178
  365.6 0.9 copy-start.10
  366.5 23.5 %collective-permute-start.6 = (bf16[1408,256]{1,0:T(8,128)(2,1)S(1)}, bf16[1408,256]{1,0:T(8,128)(2,1)}, u32[]{:S(2)}, u32[]{:S(2)}) collective-permute-start(bf16[1408,256]{1,0:T(8,128)(2,1)S(1)} %collective-permute-done.5), channel_id=1, source_target_pairs={{0,4},{4,8},{8,12},{12,16},{16,20},{20,24},{24,28},{28,0},{1,5},{5... | collective-permute-start | bytes 2162696 | tf_op jit(solution)/shard_map/ppermute | solution.py:178
  390.1 32.3 %collective-permute-start.7 = (bf16[1408,256]{1,0:T(8,128)(2,1)}, bf16[1408,256]{1,0:T(8,128)(2,1)}, u32[]{:S(2)}, u32[]{:S(2)}) collective-permute-start(bf16[1408,256]{1,0:T(8,128)(2,1)} %collective-permute-done.6), channel_id=1, source_target_pairs={{0,4},{4,8},{8,12},{12,16},{16,20},{20,24},{24,28},{28,0},{1,5},{5... | collective-permute-start | bytes 2162696 | tf_op jit(solution)/shard_map/ppermute | solution.py:178
  390.1 51.2 %copy-start.11 = (bf16[1408,256]{1,0:T(8,128)(2,1)S(1)}, bf16[1408,256]{1,0:T(8,128)(2,1)}, u32[]{:S(2)}) copy-start(bf16[1408,256]{1,0:T(8,128)(2,1)} %copy-done.10) | copy-start | bytes 2162692
  390.1 52.2 %copy-start.9 = (bf16[1408,256]{1,0:T(8,128)(2,1)S(1)}, bf16[1408,256]{1,0:T(8,128)(2,1)}, u32[]{:S(2)}) copy-start(bf16[1408,256]{1,0:T(8,128)(2,1)} %copy-done.8) | copy-start | bytes 2162692
  390.1 53.1 %copy-start.7 = (bf16[1408,256]{1,0:T(8,128)(2,1)S(1)}, bf16[1408,256]{1,0:T(8,128)(2,1)}, u32[]{:S(2)}) copy-start(bf16[1408,256]{1,0:T(8,128)(2,1)} %copy-done.6) | copy-start | bytes 2162692
  390.1 54.1 %copy-start.5 = (bf16[1408,256]{1,0:T(8,128)(2,1)S(1)}, bf16[1408,256]{1,0:T(8,128)(2,1)}, u32[]{:S(2)}) copy-start(bf16[1408,256]{1,0:T(8,128)(2,1)} %copy-done.4) | copy-start | bytes 2162692
  454.1 69.6 %copy-start.2 = (bf16[96,2048]{1,0:T(8,128)(2,1)S(1)}, bf16[96,2048]{1,0:T(8,128)(2,1)}, u32[]{:S(2)}) copy-start(bf16[96,2048]{1,0:T(8,128)(2,1)} %reduce-scatter.3.cloned.1.call-done) | copy-start | bytes 1179652
Sparse Core Ops, SparseCore 0:
  178.6 31.7 reduce-scatter.2
  213.7 19.6 all-gather.3
  235.6 133.4 all-gather.5
  371.1 114.5 all-gather.7
  497.5 26.1 reduce-scatter.4
